TPU v7x, 512 devices: a whole 4x4x16 slice. The times are simulated.
512 devices in a mesh: sp: 64 (over z, y), tp: 8 (over x, core).
Axes of the slice: x: 4, y: 4, z: 16, core: 2. Of those that a mesh axis runs over, the one named last changes fastest.
Arguments:
- queries: bfloat16 [8192, 1024], P('sp', 'tp'), may hold values from -6 to 6
- attn_out: bfloat16 [8192, 1024], P('sp', 'tp'), may hold values from -6 to 6
- out_grad: bfloat16 [8192, 1024], P('sp', 'tp'), may hold values from -384 to 384
- row_lse: float32 [8192, 8], P('sp', 'tp'), may hold values from 9.5 to 12.5
- source: bfloat16 [32768, 4096], P('sp', 'tp'), may hold values from -6 to 6
- saved_keys: bfloat16 [32768, 256], P('sp'), may hold values from -6 to 6
- saved_values: bfloat16 [32768, 256], P('sp'), may hold values from -6 to 6
- key_weight: bfloat16 [4096, 256], P('tp'), may hold values from -0.09375 to 0.09375
- value_weight: bfloat16 [4096, 256], P('tp'), may hold values from -0.09375 to 0.09375
Outputs:
- query_grad: float32 [8192, 1024], P('sp', 'tp')
- source_grad: float32 [32768, 4096], P('sp', 'tp')
- key_grad: float32 [256, 4096], P('sp', 'tp')
All inputs are finite; a program needn't handle non-finite values.
Results may differ from a plain program's by a relative error of at most 0.012.
Values may be sent and summed in bfloat16 or wider, within the bound.
No kernel may reach another device: no remote copies, remote signals or barrier semaphores. Data moves between devices by JAX's collectives and lax.ppermute only.
A program may use at most 64 MiB of HBM per device.

v0:
```python
import math
import jax
import jax.numpy as jnp
from jax import lax
from jax.sharding import Mesh
from jax.sharding import PartitionSpec as P

HEADS = 8
KV_HEADS = 2
HEAD_DIM = 128
SP = ("sp_0", "sp_1")


def copy_for_each(value, axis):
    size = lax.axis_size(axis)
    return lax.all_to_all(
        jnp.broadcast_to(value[None], (size, *value.shape)), axis, 0, 0, tiled=True
    )


def joined_along(pieces, dim):
    pieces = jnp.moveaxis(pieces, 0, dim)
    lengths = pieces.shape
    return pieces.reshape(*lengths[:dim], lengths[dim] * lengths[dim + 1], *lengths[dim + 2 :])


def gather_directly(value, axis, dim):
    pieces = copy_for_each(value, axis)
    return joined_along(pieces, dim)


def gather_axes(value, axes, dim):
    for axis in reversed(axes):
        value = lax.all_gather(value, axis, axis=dim, tiled=True)
    return value


def together(arrays, axis):
    ends = [0]
    for a in arrays:
        ends.append(ends[-1] + a.size)
    subtotal = lax.psum(jnp.concatenate([a.ravel() for a in arrays]), axis)
    return tuple((subtotal[b:e].reshape(a.shape) for a, b, e in zip(arrays, ends, ends[1:])))


def split_up(value, dim, size):
    before, after = (value.shape[:dim], value.shape[dim + 1 :])
    return jnp.moveaxis(value.reshape(*before, size, -1, *after), dim, 0)


def sum_at_owner(value, axis, dim):
    pieces = split_up(value, dim, lax.axis_size(axis))
    arrived = lax.all_to_all(pieces, axis, split_axis=0, concat_axis=0, tiled=True)
    return arrived.astype(jnp.float32).sum(axis=0)


def contract_rows(left, right):
    return lax.dot_general(
        left, right, (((0,), (0,)), ((), ())), preferred_element_type=jnp.float32
    )


def contract_cols(left, right):
    return lax.dot_general(
        left, right, (((1,), (1,)), ((), ())), preferred_element_type=jnp.float32
    )


def shards(
    queries, attn_out, out_grad, row_lse, source, saved_keys, saved_values, key_weight, value_weight
):
    local_heads = row_lse.shape[1]
    tgt_rows = queries.shape[0]
    width = queries.shape[1]
    src_rows = source.shape[0]
    sp_count = lax.axis_size(SP)
    first_head = lax.axis_index("tp") * local_heads
    per_key = HEADS // KV_HEADS
    score_scale = 1.0 / math.sqrt(HEAD_DIM)
    row_delta = jnp.sum(
        (out_grad.astype(jnp.float32) * attn_out.astype(jnp.float32)).reshape(
            tgt_rows, local_heads, HEAD_DIM
        ),
        axis=2,
    )
    row_blocks = jnp.stack([queries, out_grad])
    row_stats = jnp.stack([row_lse, row_delta])
    whole_stats = gather_directly(row_stats, SP, 1)
    kv_starts = [(first_head + 0) // per_key * HEAD_DIM]
    key_heads = [lax.dynamic_slice_in_dim(saved_keys, start, HEAD_DIM, 1) for start in kv_starts]
    value_heads = [
        lax.dynamic_slice_in_dim(saved_values, start, HEAD_DIM, 1) for start in kv_starts
    ]
    total_rows = tgt_rows * sp_count
    initial = (
        jnp.zeros((total_rows, width), jnp.float32),
        jnp.zeros((src_rows, KV_HEADS * HEAD_DIM), jnp.float32),
        jnp.zeros((src_rows, KV_HEADS * HEAD_DIM), jnp.float32),
    )
    blocks = gather_axes(row_blocks, SP, 1)
    rows = blocks.shape[1]
    span = math.gcd(rows, 1024)
    count = rows // span

    def step(turn, inner):
        query_buf, key_acc, value_acc = inner
        begin = turn * span
        block_rows = lax.dynamic_slice_in_dim(blocks, begin, span, 1)
        block_stats = lax.dynamic_slice_in_dim(whole_stats, begin, span, 1)
        query_head = block_rows[0, :, 0:HEAD_DIM]
        grad_head = block_rows[1, :, 0:HEAD_DIM]
        lse_col = block_stats[0, :, 0:1]
        delta_col = block_stats[1, :, 0:1]
        scores = contract_cols(query_head, key_heads[0]) * score_scale
        attn_probs = jnp.exp(scores - lse_col)
        dprobs = contract_cols(grad_head, value_heads[0])
        dscores = (attn_probs * (dprobs - delta_col) * score_scale).astype(jnp.bfloat16)
        parts = [jnp.dot(dscores, key_heads[0], preferred_element_type=jnp.float32)]
        key_part = contract_rows(dscores, query_head)
        value_part = contract_rows(attn_probs.astype(jnp.bfloat16), grad_head)
        kv_start = kv_starts[0]
        key_acc = lax.dynamic_update_slice_in_dim(
            key_acc,
            lax.dynamic_slice_in_dim(key_acc, kv_start, HEAD_DIM, 1) + key_part,
            kv_start,
            1,
        )
        value_acc = lax.dynamic_update_slice_in_dim(
            value_acc,
            lax.dynamic_slice_in_dim(value_acc, kv_start, HEAD_DIM, 1) + value_part,
            kv_start,
            1,
        )
        query_buf = lax.dynamic_update_slice_in_dim(
            query_buf, jnp.concatenate(parts, axis=1), begin, 0
        )
        return (query_buf, key_acc, value_acc)

    partials, key_acc, value_acc = lax.fori_loop(0, count, step, initial)
    stacked = partials.reshape(sp_count, tgt_rows, width)
    received = lax.all_to_all(
        stacked.astype(jnp.bfloat16), SP, split_axis=0, concat_axis=0, tiled=True
    ).astype(stacked.dtype)
    query_grad = jnp.sum(received, axis=0)
    key_acc, value_acc = tuple(
        (
            part.astype(jnp.float32)
            for part in together(
                (key_acc.astype(jnp.bfloat16), value_acc.astype(jnp.bfloat16)), "tp"
            )
        )
    )
    key_half = key_acc.astype(jnp.bfloat16)
    value_half = value_acc.astype(jnp.bfloat16)
    source_grad = contract_cols(key_half, key_weight) + contract_cols(value_half, value_weight)
    weight_scale = 1.0 / math.sqrt(src_rows * sp_count)
    key_grad = sum_at_owner(
        (contract_rows(key_half, source) * weight_scale).astype(jnp.bfloat16), SP, 0
    )
    return (query_grad, source_grad, key_grad)


def solution(mesh):
    split = Mesh(mesh.devices.reshape(16, 4, mesh.shape["tp"]), ("sp_0", "sp_1", "tp"))
    return jax.shard_map(
        shards,
        mesh=split,
        in_specs=(
            P(SP, "tp"),
            P(SP, "tp"),
            P(SP, "tp"),
            P(SP, "tp"),
            P(SP, "tp"),
            P(SP, None),
            P(SP, None),
            P("tp", None),
            P("tp", None),
        ),
        out_specs=(P(SP, "tp"), P(SP, "tp"), P(SP, "tp")),
        check_vma=False,
    )
```

profile of v0, /device:TPU:6, one launch (start us, length us, event | category | flops | bytes accessed | tf_op | source)
XLA Modules:
  0.0 390.1 jit_solution(9942946184266667918)
XLA Ops:
  8.1 13.5 %all_gather.6 = bf16[2,512,128]{2,1,0:T(8,128)(2,1)} all-gather(bf16[2,128,128]{2,1,0:T(8,128)(2,1)S(1)} %pad_maximum_fusion.1), channel_id=1, replica_groups=mesh['sp_0'=16,'sp_1'=4,'tp'=8] {'sp_1'}, dimensions={1}, use_global_device_ids=true | all-gather | bytes 327680 | tf_op jit(solution)/shard_map/all_gather | solution.py:34
  23.8 18.2 %all-to-all-start = ((f32[64,2,128,1]{2,1,3,0:T(2,128)}), f32[64,2,128,1]{2,1,3,0:T(2,128)S(1)}, u32[]{:S(2)}, u32[]{:S(2)}) async-start(f32[64,2,128,1]{2,1,3,0:T(2,128)} %broadcast_in_dim.13), calls=%async_computation | async-start | bytes 131072 | tf_op jit(solution)/shard_map/all_to_all | solution.py:16
  43.0 14.7 %all-to-all-done = f32[64,2,128,1]{2,1,3,0:T(2,128)S(1)} async-done(((f32[64,2,128,1]{2,1,3,0:T(2,128)}), f32[64,2,128,1]{2,1,3,0:T(2,128)S(1)}, u32[]{:S(2)}, u32[]{:S(2)}) %all-to-all-start) | async-done | bytes 65568 | tf_op jit(solution)/shard_map/all_to_all | solution.py:16
  57.8 47.4 %all-gather.2.cloned.1.call-done = bf16[2,8192,128]{2,1,0:T(8,128)(2,1)} async-done(((bf16[2,512,128]{2,1,0:T(8,128)(2,1)}), bf16[2,8192,128]{2,1,0:T(8,128)(2,1)}) %all-gather.2.cloned.1.call-update) | async-done | bytes 4194320 | tf_op jit(solution)/shard_map/all_gather | solution.py:34
  106.7 58.4 %while.19 = (s32[]{:T(128)}, bf16[8192,128]{1,0:T(8,128)(2,1)}, f32[512,256]{1,0:T(8,128)S(1)}, f32[512,256]{1,0:T(8,128)S(1)}, bf16[2,8192,128]{2,1,0:T(8,128)(...) while((s32[]{:T(128)}, bf16[8192,128]{1,0:T(8,128)(2,1)}, ...), condition=%wide.region_2.3_spmd, body=%wide.region_1.2_spmd.sunk | while | flops 675938304 | bytes 12481763 | solution.py:139
  108.1 1.7 fusion.43
  109.8 1.6 multiply_convert_fusion.2
  115.4 1.7 fusion.43
  122.7 1.7 fusion.43
  124.4 1.6 multiply_convert_fusion.2
  130.0 1.7 fusion.43
  131.7 1.6 multiply_convert_fusion.2
  137.4 1.7 fusion.43
  139.1 1.6 multiply_convert_fusion.2
  144.6 1.7 fusion.43
  151.9 1.7 fusion.43
  153.6 1.6 multiply_convert_fusion.2
  159.2 1.7 fusion.43
  160.9 1.6 multiply_convert_fusion.2
  166.5 70.1 %all-reduce.2.cloned.1.call-done = bf16[262144]{0:T(1024)(128)(2,1)} async-done(((bf16[262144]{0:T(1024)(128)(2,1)}), bf16[262144]{0:T(1024)(128)(2,1)}) %all-reduce.2.cloned.1.call-update) | async-done | bytes 524304 | tf_op jit(solution)/shard_map/psum | solution.py:42
  238.6 38.4 %all_to_all.15 = bf16[64,4,512]{2,1,0:T(4,128)(2,1)S(1)} all-to-all(bf16[64,4,512]{2,1,0:T(4,128)(2,1)S(1)} %reshape.49), channel_id=1, replica_groups=mesh['sp_0'=16,'sp_1'=4,'tp'=8] {'sp_0','sp_1'}, dimensions={0} | all-to-all | bytes 524288 | tf_op jit(solution)/shard_map/all_to_all | solution.py:53
  277.0 5.4 %all-to-all-start.1 = ((bf16[64,128,128]{2,1,0:T(8,128)(2,1)}), bf16[64,128,128]{2,1,0:T(8,128)(2,1)S(1)}, u32[]{:S(2)}, u32[]{:S(2)}) async-start(bf16[64,128,128]{2,1,0:T(8,128)(2,1)} %bitcast.58), calls=%async_computation.1 | async-start | bytes 4194304 | tf_op jit(solution)/shard_map/all_to_all | solution.py:141
  283.9 2.3 convolution_add_fusion.2
  286.8 95.4 %all-to-all-done.1 = bf16[64,128,128]{2,1,0:T(8,128)(2,1)S(1)} async-done(((bf16[64,128,128]{2,1,0:T(8,128)(2,1)}), bf16[64,128,128]{2,1,0:T(8,128)(2,1)S(1)}, u32[]{:S(2)}, u32[]{:S(2)}) %all-to-all-start.1) | async-done | bytes 2097184 | tf_op jit(solution)/shard_map/all_to_all | solution.py:141
  (64 shorter events, 46.9 us)
Async XLA Ops:
  7.2 230.6 %copy-start = (bf16[512,512]{1,0:T(8,128)(2,1)S(1)}, bf16[512,512]{1,0:T(8,128)(2,1)}, u32[]{:S(2)}) copy-start(bf16[512,512]{1,0:T(8,128)(2,1)} %param.15) | copy-start | bytes 1572868
  7.2 98.0 %all-gather.2.cloned.1.call-start = ((), (), s32[]{:S(2)}) async-start(), calls=%async_computation.3 | async-start | bytes 4456448 | tf_op jit(solution)/shard_map/all_gather | solution.py:34
  23.8 34.0 %all-to-all-start = ((f32[64,2,128,1]{2,1,3,0:T(2,128)}), f32[64,2,128,1]{2,1,3,0:T(2,128)S(1)}, u32[]{:S(2)}, u32[]{:S(2)}) async-start(f32[64,2,128,1]{2,1,3,0:T(2,128)} %broadcast_in_dim.13), calls=%async_computation | async-start | bytes 131072 | tf_op jit(solution)/shard_map/all_to_all | solution.py:16
  42.0 194.6 %all-reduce.2.cloned.1.call-start = ((), (), s32[]{:S(2)}) async-start(), calls=%async_computation.4 | async-start | bytes 1048576 | tf_op jit(solution)/shard_map/psum | solution.py:42
  237.8 0.7 copy-start.1
  277.0 105.3 %all-to-all-start.1 = ((bf16[64,128,128]{2,1,0:T(8,128)(2,1)}), bf16[64,128,128]{2,1,0:T(8,128)(2,1)S(1)}, u32[]{:S(2)}, u32[]{:S(2)}) async-start(bf16[64,128,128]{2,1,0:T(8,128)(2,1)} %bitcast.58), calls=%async_computation.1 | async-start | bytes 4194304 | tf_op jit(solution)/shard_map/all_to_all | solution.py:141
Sparse Core Ops, SparseCore 0:
  21.7 83.4 all-gather.1
  166.6 69.9 all-reduce.1
where the time goes:
time: 392 us; the launch traced here: 390 us
  waiting for transfers between devices  228 us (58%)
  matrix products  62.1 us (16%)
  blocking collectives  51.9 us (13%)
  starting transfers between devices  23.6 us (6%)
  between operations  14.2 us (4%)
  local copies, waits for them, and re-layouts  5.3 us (1%)
  other arithmetic  4.95 us (1%)
    all_to_all x1, waiting for transfers between devices, shards(): lax.all_to_all(stacked.astype(jnp.bfloat16), SP, split_axis=0, concat_axi...  95.4 us
    psum x1, waiting for transfers between devices, together(): subtotal = lax.psum(jnp.concatenate([a.ravel() for a in arrays]), axis)  70.1 us
    all_gather x1, waiting for transfers between devices, gather_axes(): value = lax.all_gather(value, axis, axis=dim, tiled=True)  47.4 us
    all_to_all x1, blocking collectives, sum_at_owner(): lax.all_to_all(pieces, axis, split_axis=0, concat_axis=0, tiled=True)  38.4 us
    dot_general x18, matrix products, contract_cols(): lax.dot_general(left, right, (((1,), (1,)), ((), ())), preferred_element_...  27.6 us
    dot_general x17, matrix products, contract_rows(): lax.dot_general(left, right, (((0,), (0,)), ((), ())), preferred_element_...  25.4 us
    all_to_all x1, starting transfers between devices, copy_for_each(): lax.all_to_all(jnp.broadcast_to(value[None], (size, *value.shape)), axis,...  18.2 us
    all_to_all x1, waiting for transfers between devices, copy_for_each(): lax.all_to_all(jnp.broadcast_to(value[None], (size, *value.shape)), axis,...  14.7 us
  transfers between devices with their start and end apart: 4, of which 4 were waited for; matrix products, arithmetic and copies ran while one was open for 2% of the time, Pallas kernels for 0%

commit v1 on v0

--- a/solution.py
+++ b/solution.py
@@ -39,7 +39,9 @@
     ends = [0]
     for a in arrays:
         ends.append(ends[-1] + a.size)
-    subtotal = lax.psum(jnp.concatenate([a.ravel() for a in arrays]), axis)
+    part_2 = jnp.concatenate([a.ravel() for a in arrays])
+    cells = lax.all_gather(part_2, axis, axis=0, tiled=False)
+    subtotal = cells.sum(axis=0)
     return tuple((subtotal[b:e].reshape(a.shape) for a, b, e in zip(arrays, ends, ends[1:])))
 
 

time: 392 us -> 302 us (0.77)
  waiting for transfers between devices: 228 us -> 148 us
  blocking collectives: 51.9 us -> 13.5 us
  starting transfers between devices: 23.6 us -> 34.4 us
  other arithmetic: 4.95 us -> 15.3 us
  local copies, waits for them, and re-layouts: 5.3 us -> 12.2 us
    psum x1 -> x0, waiting for transfers between devices: 70.1 us -> none  [together(): subtotal = lax.psum(jnp.concatenate([a.ravel() for a in arrays]), axis)]
    all_to_all x1, waiting for transfers between devices: 95.4 us -> 48.2 us  [shards(): lax.all_to_all(stacked.astype(jnp.bfloat16), SP, split_axis=0, concat_axi...]
    all_to_all x1 -> x0, blocking collectives: 38.4 us -> none  [sum_at_owner(): lax.all_to_all(pieces, axis, split_axis=0, concat_axis=0, tiled=True)]
    all_gather x0 -> x1, waiting for transfers between devices: none -> 23.5 us  [together(): cells = lax.all_gather(part_2, axis, axis=0, tiled=False)]
    all_to_all x0 -> x1, waiting for transfers between devices: none -> 14 us  [sum_at_owner(): lax.all_to_all(pieces, axis, split_axis=0, concat_axis=0, tiled=True)]
    reduce_sum x0 -> x1, other arithmetic: none -> 10.3 us  [together(): subtotal = cells.sum(axis=0)]
    all_gather x0 -> x1, local copies, waits for them, and re-layouts: none -> 5.92 us  [together(): cells = lax.all_gather(part_2, axis, axis=0, tiled=False)]
    all_to_all x0 -> x1, starting transfers between devices: none -> 5.84 us  [sum_at_owner(): lax.all_to_all(pieces, axis, split_axis=0, concat_axis=0, tiled=True)]
  transfers between devices with their start and end apart: 4 -> 5, of which waited for: 4 -> 5; matrix products, arithmetic and copies ran while one was open for 2% -> 9% of each run, Pallas kernels for 0% -> 0%
where the time goes in v1:
time: 302 us; the launch traced here: 300 us
  waiting for transfers between devices  148 us (49%)
  matrix products  62.7 us (21%)
  starting transfers between devices  34.4 us (11%)
  other arithmetic  15.3 us (5%)
  between operations  14.2 us (5%)
  blocking collectives  13.5 us (4%)
  local copies, waits for them, and re-layouts  12.2 us (4%)
    all_to_all x1, waiting for transfers between devices, shards(): lax.all_to_all(stacked.astype(jnp.bfloat16), SP, split_axis=0, concat_axi...  48.2 us
    all_gather x1, waiting for transfers between devices, gather_axes(): value = lax.all_gather(value, axis, axis=dim, tiled=True)  47.4 us
    dot_general x18, matrix products, contract_cols(): lax.dot_general(left, right, (((1,), (1,)), ((), ())), preferred_element_...  27.9 us
    dot_general x17, matrix products, contract_rows(): lax.dot_general(left, right, (((0,), (0,)), ((), ())), preferred_element_...  25.7 us
    all_gather x1, waiting for transfers between devices, together(): cells = lax.all_gather(part_2, axis, axis=0, tiled=False)  23.5 us
    all_to_all x1, starting transfers between devices, copy_for_each(): lax.all_to_all(jnp.broadcast_to(value[None], (size, *value.shape)), axis,...  18.2 us
    all_to_all x1, waiting for transfers between devices, copy_for_each(): lax.all_to_all(jnp.broadcast_to(value[None], (size, *value.shape)), axis,...  14.7 us
    all_to_all x1, waiting for transfers between devices, sum_at_owner(): lax.all_to_all(pieces, axis, split_axis=0, concat_axis=0, tiled=True)  14 us
  transfers between devices with their start and end apart: 5, of which 5 were waited for; matrix products, arithmetic and copies ran while one was open for 9% of the time, Pallas kernels for 0%

profile of v1, /device:TPU:6, one launch (start us, length us, event | category | flops | bytes accessed | tf_op | source)
XLA Modules:
  0.0 300.4 jit_solution(15039779766509774132)
XLA Ops:
  8.1 13.5 %all_gather.12 = bf16[2,512,128]{2,1,0:T(8,128)(2,1)} all-gather(bf16[2,128,128]{2,1,0:T(8,128)(2,1)S(1)} %pad_maximum_fusion.1), channel_id=1, replica_groups=mesh['sp_0'=16,'sp_1'=4,'tp'=8] {'sp_1'}, dimensions={1}, use_global_device_ids=true | all-gather | bytes 327680 | tf_op jit(solution)/shard_map/all_gather | solution.py:34
  23.8 18.2 %all-to-all-start = ((f32[64,2,128,1]{2,1,3,0:T(2,128)}), f32[64,2,128,1]{2,1,3,0:T(2,128)S(1)}, u32[]{:S(2)}, u32[]{:S(2)}) async-start(f32[64,2,128,1]{2,1,3,0:T(2,128)} %broadcast_in_dim.13), calls=%async_computation | async-start | bytes 131072 | tf_op jit(solution)/shard_map/all_to_all | solution.py:16
  43.0 14.7 %all-to-all-done = f32[64,2,128,1]{2,1,3,0:T(2,128)S(1)} async-done(((f32[64,2,128,1]{2,1,3,0:T(2,128)}), f32[64,2,128,1]{2,1,3,0:T(2,128)S(1)}, u32[]{:S(2)}, u32[]{:S(2)}) %all-to-all-start) | async-done | bytes 65568 | tf_op jit(solution)/shard_map/all_to_all | solution.py:16
  57.8 47.4 %all-gather.4.cloned.1.call-done = bf16[2,8192,128]{2,1,0:T(8,128)(2,1)} async-done(((bf16[2,512,128]{2,1,0:T(8,128)(2,1)}), bf16[2,8192,128]{2,1,0:T(8,128)(2,1)}) %all-gather.4.cloned.1.call-update) | async-done | bytes 4194320 | tf_op jit(solution)/shard_map/all_gather | solution.py:34
  106.8 59.0 %while.19 = (s32[]{:T(128)}, bf16[8192,128]{1,0:T(8,128)(2,1)}, f32[512,256]{1,0:T(8,128)S(1)}, f32[512,256]{1,0:T(8,128)S(1)}, bf16[2,8192,128]{2,1,0:T(8,128)(...) while((s32[]{:T(128)}, bf16[8192,128]{1,0:T(8,128)(2,1)}, ...), condition=%wide.region_2.3_spmd, body=%wide.region_1.2_spmd.sunk | while | flops 675938304 | bytes 12481763 | solution.py:141
  108.2 1.7 fusion.43
  115.5 1.7 fusion.43
  117.3 1.7 multiply_convert_fusion.2
  122.9 1.7 fusion.43
  124.6 1.7 multiply_convert_fusion.2
  130.3 1.7 fusion.43
  132.0 1.7 multiply_convert_fusion.2
  137.7 1.7 fusion.43
  145.0 1.7 fusion.43
  152.4 1.7 fusion.43
  159.7 1.7 fusion.43
  167.1 10.3 %all-to-all-start.1 = ((bf16[64,128,128]{2,1,0:T(8,128)(2,1)}), bf16[64,128,128]{2,1,0:T(8,128)(2,1)S(1)}, u32[]{:S(2)}, u32[]{:S(2)}) async-start(bf16[64,128,128]{2,1,0:T(8,128)(2,1)} %bitcast.58), calls=%async_computation.1 | async-start | bytes 4194304 | tf_op jit(solution)/shard_map/all_to_all | solution.py:143
  177.4 23.5 %all-gather.6.cloned.1.call-done = bf16[2097152]{0:T(1024)(128)(2,1)} async-done(((bf16[262144]{0:T(1024)(128)(2,1)}), bf16[2097152]{0:T(1024)(128)(2,1)}) %all-gather.6.cloned.1.call-update) | async-done | bytes 4194320 | tf_op jit(solution)/shard_map/all_gather | solution.py:43
  200.9 5.9 %reshape.50 = bf16[8,262144]{1,0:T(8,128)(2,1)} reshape(bf16[2097152]{0:T(1024)(128)(2,1)} %all-gather.6.cloned.1.call-done) | data formatting | bytes 8388608 | tf_op jit(solution)/shard_map/all_gather | solution.py:43
  206.8 10.3 %reduce_sum.41 = bf16[262144]{0:T(1024)(128)(2,1)S(1)} reduce(bf16[8,262144]{1,0:T(8,128)(2,1)} %reshape.50, bf16[]{:T(256)} %constant.86.clone.1), dimensions={0}, to_apply=%region_4.5 | reduce | flops 1835008 | bytes 4718594 | tf_op jit(solution)/shard_map/reduce_sum | solution.py:44
  220.0 48.2 %all-to-all-done.1 = bf16[64,128,128]{2,1,0:T(8,128)(2,1)S(1)} async-done(((bf16[64,128,128]{2,1,0:T(8,128)(2,1)}), bf16[64,128,128]{2,1,0:T(8,128)(2,1)S(1)}, u32[]{:S(2)}, u32[]{:S(2)}) %all-to-all-start.1) | async-done | bytes 2097184 | tf_op jit(solution)/shard_map/all_to_all | solution.py:143
  268.3 5.8 %all-to-all-start.2 = ((bf16[64,4,512]{2,1,0:T(4,128)(2,1)}), bf16[64,4,512]{2,1,0:T(4,128)(2,1)S(1)}, u32[]{:S(2)}, u32[]{:S(2)}) async-start(bf16[64,4,512]{2,1,0:T(4,128)(2,1)} %reshape.49), calls=%async_computation.2 | async-start | bytes 524288 | tf_op jit(solution)/shard_map/all_to_all | solution.py:55
  275.6 2.3 convolution_add_fusion.2
  278.8 14.0 %all-to-all-done.2 = bf16[64,4,512]{2,1,0:T(4,128)(2,1)S(1)} async-done(((bf16[64,4,512]{2,1,0:T(4,128)(2,1)}), bf16[64,4,512]{2,1,0:T(4,128)(2,1)S(1)}, u32[]{:S(2)}, u32[]{:S(2)}) %all-to-all-start.2) | async-done | bytes 262176 | tf_op jit(solution)/shard_map/all_to_all | solution.py:55
  (67 shorter events, 53.0 us)
Async XLA Ops:
  7.2 211.8 %copy-start = (bf16[512,512]{1,0:T(8,128)(2,1)S(1)}, bf16[512,512]{1,0:T(8,128)(2,1)}, u32[]{:S(2)}) copy-start(bf16[512,512]{1,0:T(8,128)(2,1)} %param.15) | copy-start | bytes 1572868
  7.2 98.0 %all-gather.4.cloned.1.call-start = ((), (), s32[]{:S(2)}) async-start(), calls=%async_computation.3 | async-start | bytes 4456448 | tf_op jit(solution)/shard_map/all_gather | solution.py:34
  23.8 34.0 %all-to-all-start = ((f32[64,2,128,1]{2,1,3,0:T(2,128)}), f32[64,2,128,1]{2,1,3,0:T(2,128)S(1)}, u32[]{:S(2)}, u32[]{:S(2)}) async-start(f32[64,2,128,1]{2,1,3,0:T(2,128)} %broadcast_in_dim.13), calls=%async_computation | async-start | bytes 131072 | tf_op jit(solution)/shard_map/all_to_all | solution.py:16
  42.0 158.9 %all-gather.6.cloned.1.call-start = ((), (), s32[]{:S(2)}) async-start(), calls=%async_computation.4 | async-start | bytes 4718592 | tf_op jit(solution)/shard_map/all_gather | solution.py:43
  167.1 101.2 %all-to-all-start.1 = ((bf16[64,128,128]{2,1,0:T(8,128)(2,1)}), bf16[64,128,128]{2,1,0:T(8,128)(2,1)S(1)}, u32[]{:S(2)}, u32[]{:S(2)}) async-start(bf16[64,128,128]{2,1,0:T(8,128)(2,1)} %bitcast.58), calls=%async_computation.1 | async-start | bytes 4194304 | tf_op jit(solution)/shard_map/all_to_all | solution.py:143
  218.9 55.2 %copy-start.1 = (bf16[512,256]{1,0:T(8,128)(2,1)}, bf16[512,256]{1,0:T(8,128)(2,1)S(1)}, u32[]{:S(2)}) copy-start(bf16[512,256]{1,0:T(8,128)(2,1)S(1)} %slice.63) | copy-start | bytes 786436
  268.3 24.5 %all-to-all-start.2 = ((bf16[64,4,512]{2,1,0:T(4,128)(2,1)}), bf16[64,4,512]{2,1,0:T(4,128)(2,1)S(1)}, u32[]{:S(2)}, u32[]{:S(2)}) async-start(bf16[64,4,512]{2,1,0:T(4,128)(2,1)} %reshape.49), calls=%async_computation.2 | async-start | bytes 524288 | tf_op jit(solution)/shard_map/all_to_all | solution.py:55
Sparse Core Ops, SparseCore 0:
  21.7 83.4 all-gather.3
  167.2 33.6 all-gather.5
